TPU v7x, 256 devices: a 4x2x16 block of a 4x16x16 slice. The times are simulated.
256 devices in a mesh: grp: 2 (over y), sp: 32 (over z, core), tp: 4 (over x).
Axes of the slice: x: 4, y: 2, z: 16, core: 2. Of those that a mesh axis runs over, the one named last changes fastest.
The devices are a block of a 4x16x16 slice.
Arguments:
- carryover_vector: bfloat16 [16384, 2048], P(('grp', 'sp', 'tp')), parts along dimension 0, may hold values from -6 to 6
- channel_source_entries: bfloat16 [16384, 1024], P(('grp', 'sp'), 'tp'), parts along dimension 0, may hold values from -6 to 6
- final_modulation_vector: bfloat16 [16384, 1024], P(('grp', 'sp'), 'tp'), parts along dimension 0, may hold values from -54 to 54
- entering_basis_matrix: bfloat16 [16384, 512], P(('grp', 'sp'), 'tp'), parts along dimension 0, may hold values from -6 to 6
- readout_basis_matrix: bfloat16 [16384, 512], P(('grp', 'sp'), 'tp'), parts along dimension 0, may hold values from -6 to 6
- raw_stride_amount: float32 [16384, 16], P(('grp', 'sp'), 'tp'), parts along dimension 0, may hold values from -6 to 5
- extra_log_attenuation: float32 [16384, 16], P(('grp', 'sp'), 'tp'), parts along dimension 0, may hold values from -1.4 to 0
- channel_fading_rate: float32 [16], P('tp'), may hold values from 0 to 0.1, as said below
- channel_source_kernel: float32 [4, 1024], P(None, 'tp'), may hold values from -3 to 3
- entering_basis_kernel: float32 [4, 512], P(None, 'tp'), may hold values from -3 to 3
- readout_basis_kernel: float32 [4, 512], P(None, 'tp'), may hold values from -3 to 3
- modulated_rescaling_vector: float32 [1024], replicated, may hold values from 0.1 to 1.9
- blender_final_matrix: bfloat16 [1024, 2048], replicated, may hold values from -0.1875 to 0.1875
- specialist_rescaling_vector: float32 [2048], replicated, may hold values from 0.1 to 1.9
- specialist_gating_matrices: bfloat16 [64, 2048, 1024], P('sp', None, 'tp'), may hold values from -0.125 to 0.125
- widening_matrices: bfloat16 [64, 2048, 1024], P('sp', None, 'tp'), may hold values from -0.125 to 0.125
- contracting_matrices: bfloat16 [64, 1024, 2048], P('sp', 'tp'), may hold values from -0.1875 to 0.1875
- assigned_specialist_ids: int32 [16384, 2], P(('grp', 'sp')), parts along dimension 0, may hold values from 0 to 63, as said below
- specialist_choice_affinity: float32 [16384, 2], P(('grp', 'sp', 'tp')), parts along dimension 0, may hold values from -6 to 6
- cluster_chance: float32 [16384], P(('grp', 'sp', 'tp')), parts along dimension 0, may hold values from 0.25 to 1
Outputs:
- layer_out: bfloat16 [16384, 2048], P(('grp', 'sp', 'tp')), parts along dimension 0
There are 2 independent parts, one for each index of `grp`. A program takes and returns all parts, laid end to end along the dimension named above; an argument that names none is the same for every part. Nothing has to cross between parts.
Inputs may be any that keep to these rules, and one draw needn't show every extreme that they name: `assigned_specialist_ids`: each row names 2 different experts of one group: the experts g * 16 to (g + 1) * 16 - 1 for one g below 4. In each aligned block of 64 rows (the rows of one device) no expert is named by more than 4 rows, and every expert of one group, the same group in all blocks, is named by exactly 4 rows of every block. `channel_fading_rate`: positive.
All inputs are finite; a program needn't handle non-finite values.
Results may differ from a plain program's by a relative error of at most 0.015.
Values may be sent and summed in bfloat16 or wider, within the bound.
A program may use at most 64 MiB of HBM per device.

v0:
```python
import jax
import jax.numpy as jnp
from jax import lax
from jax.sharding import Mesh
from jax.sharding import PartitionSpec as P

HEAD_DIM = 64
STATE = 128
BLOCK = 64
SP = ("sp_0", "sp_1")
GRP_SP_TP = ("grp", "sp_0", "sp_1", "tp")
GRP_SP = ("grp", "sp_0", "sp_1")
EPS = 1e-06


def filled_with(x, identity):
    return jax.tree.map(
        lambda part, zero: jnp.zeros_like(part) + jnp.asarray(zero, part.dtype), x, identity
    )


def carried_in(x, axes, combine, identity):
    before = start = filled_with(x, identity)
    subtotal = x
    for axis in reversed(axes):
        size, index = (lax.axis_size(axis), lax.axis_index(axis))
        pieces = jax.tree.map(
            lambda part, kind: lax.all_gather(part.astype(kind), axis),
            subtotal,
            (jnp.bfloat16, jnp.bfloat16),
        )
        inside, subtotal = (start, start)
        for k in range(size):
            passed = k < index
            subtotal = combine(
                subtotal, jax.tree.map(lambda part, own: part[k].astype(own.dtype), pieces, x)
            )
            inside = jax.tree.map(lambda new, old: jnp.where(passed, new, old), subtotal, inside)
        before = combine(inside, before)
    return before


def from_behind(x, axis, by):
    size = lax.axis_size(axis)
    pairs = [(i, i + by) for i in range(size) if 0 <= i + by < size]
    return lax.ppermute(x, axis, pairs)


def for_sending(x):
    return jax.tree.map(lambda a: a.astype(jnp.bfloat16) if a.dtype == jnp.float32 else a, x)


def split_up(x, dim, size):
    shape = x.shape
    blocks = x.reshape(*shape[:dim], size, shape[dim] // size, *shape[dim + 1 :])
    return jnp.moveaxis(blocks, dim, 0)


def summed_on_arrival(x, axis, dim):
    size = lax.axis_size(axis)
    blocks = lax.all_to_all(split_up(x, dim, size), axis, 0, 0, tiled=True)
    return jnp.sum(blocks.astype(jnp.float32), axis=0)


def causal_conv(signal, earlier, weights):
    kernel_len = weights.shape[0]
    length = signal.shape[0]
    joined = jnp.concatenate([earlier, signal], axis=0).astype(jnp.float32)
    accumulated = jnp.zeros((length, signal.shape[1]), jnp.float32)
    for offset in range(kernel_len):
        accumulated = accumulated + weights[offset][None, :] * joined[offset : offset + length]
    return jax.nn.silu(accumulated)


def link_states(earlier, later):
    return (earlier[0] * later[0], earlier[1] * later[0][..., None, None] + later[1])


def device_states(scaled_in, log_attenuation, keys_b, queries_c, groups_here):
    length = scaled_in.shape[0]
    blocks = length // BLOCK
    per_group = scaled_in.shape[1] // groups_here
    scaled_in = scaled_in.reshape(blocks, BLOCK, groups_here, per_group, HEAD_DIM)
    log_attenuation = log_attenuation.reshape(blocks, BLOCK, groups_here, per_group)
    keys_b = keys_b.reshape(blocks, BLOCK, groups_here, STATE)
    queries_c = queries_c.reshape(blocks, BLOCK, groups_here, STATE)
    running = jnp.cumsum(log_attenuation, axis=1)
    lower_mask = jnp.tril(jnp.ones((BLOCK, BLOCK), dtype=bool))
    between = running[:, :, None] - running[:, None, :]
    decays = jnp.exp(jnp.where(lower_mask[None, :, :, None, None], between, -jnp.inf))
    scores = jnp.einsum("blgn,bsgn->blsg", queries_c, keys_b)
    inside = jnp.einsum("blsg,blsgr,bsgrp->blgrp", scores, decays, scaled_in)
    totals = running[:, -1]
    remain = jnp.exp(totals[:, None] - running)
    block_states = jnp.einsum("bsgn,bsgr,bsgrp->bgrpn", keys_b, remain, scaled_in)

    def advance(carried, pieces):
        return (carried * jnp.exp(pieces[1])[..., None, None] + pieces[0], carried)

    initial = jnp.zeros(block_states.shape[1:], jnp.float32)
    own_state, entering = lax.scan(advance, initial, (block_states, totals))
    own_decay = jnp.exp(jnp.sum(totals, axis=0))
    _, incoming = carried_in(
        (own_decay, own_state),
        SP,
        link_states,
        (jnp.ones_like(own_decay), jnp.zeros_like(own_state)),
    )
    preceding = jnp.exp(jnp.cumsum(totals, axis=0) - totals)
    entering = entering + preceding[..., None, None] * incoming[None]
    outside = jnp.einsum("blgn,bgrpn,blgr->blgrp", queries_c, entering, jnp.exp(running))
    return (inside + outside).reshape(length, -1)


def fetch_rows(tokens, sources):
    present = sources >= 0
    picked = jnp.take(tokens, jnp.maximum(sources, 0), axis=0)
    return jnp.where(present[:, None], picked, jnp.zeros_like(picked))


def slot_tables(chosen_ids, quarters, row_count, experts, capacity):
    picks = chosen_ids.shape[1]
    flat_ids = chosen_ids.reshape(quarters, row_count * picks)
    member = (flat_ids[..., None] == jnp.arange(experts, dtype=jnp.int32)).astype(jnp.int32)
    position = jnp.sum((jnp.cumsum(member, axis=1) - member) * member, axis=2)
    quarter_ids = jnp.arange(quarters, dtype=jnp.int32)[:, None]
    slot_index = flat_ids * (quarters * capacity) + quarter_ids * capacity + position
    token_index = (
        quarter_ids * row_count + jnp.arange(row_count * picks, dtype=jnp.int32)[None, :] // picks
    )
    sources = (
        jnp.full((experts * quarters * capacity,), -1, jnp.int32)
        .at[slot_index.reshape(-1)]
        .set(token_index.reshape(-1))
    )
    return (sources, position)


def per_device(
    carryover_vector,
    channel_source_entries,
    final_modulation_vector,
    entering_basis_matrix,
    readout_basis_matrix,
    raw_stride_amount,
    extra_log_attenuation,
    channel_fading_rate,
    channel_source_kernel,
    entering_basis_kernel,
    readout_basis_kernel,
    modulated_rescaling_vector,
    blender_final_matrix,
    specialist_rescaling_vector,
    specialist_gating_matrices,
    widening_matrices,
    contracting_matrices,
    assigned_specialist_ids,
    specialist_choice_affinity,
    cluster_chance,
):
    length = channel_source_entries.shape[0]
    row_count = carryover_vector.shape[0]
    model_width = carryover_vector.shape[1]
    heads_here = channel_fading_rate.shape[0]
    groups_here = entering_basis_matrix.shape[1] // STATE
    tp_index = lax.axis_index("tp")
    rim_rows = channel_source_kernel.shape[0] - 1
    neighbours = from_behind(
        (
            channel_source_entries[length - rim_rows :],
            entering_basis_matrix[length - rim_rows :],
            readout_basis_matrix[length - rim_rows :],
        ),
        SP,
        1,
    )
    inputs_x = causal_conv(channel_source_entries, neighbours[0], channel_source_kernel)
    keys_b = causal_conv(entering_basis_matrix, neighbours[1], entering_basis_kernel)
    queries_c = causal_conv(readout_basis_matrix, neighbours[2], readout_basis_kernel)
    channel_stride_amount = jax.nn.softplus(raw_stride_amount)
    log_attenuation = extra_log_attenuation - channel_fading_rate[None, :] * channel_stride_amount
    heads_x = inputs_x.reshape(length, heads_here, HEAD_DIM)
    mixed = device_states(
        heads_x * channel_stride_amount[:, :, None], log_attenuation, keys_b, queries_c, groups_here
    )
    gated = mixed * jax.nn.silu(final_modulation_vector.astype(jnp.float32))
    own_rows = lax.all_to_all(
        for_sending(gated), "tp", split_axis=0, concat_axis=1, tiled=True
    ).astype(gated.dtype)
    normed = (
        own_rows
        * lax.rsqrt(jnp.mean(own_rows * own_rows, axis=1, keepdims=True) + EPS)
        * modulated_rescaling_vector[None, :]
    ).astype(jnp.bfloat16)
    middle = (
        carryover_vector.astype(jnp.float32)
        + jnp.dot(normed, blender_final_matrix, preferred_element_type=jnp.float32)
    ).astype(jnp.bfloat16)
    middle_wide = middle.astype(jnp.float32)
    expert_input = (
        middle_wide
        * lax.rsqrt(jnp.mean(middle_wide * middle_wide, axis=1, keepdims=True) + EPS)
        * specialist_rescaling_vector[None, :]
    ).astype(jnp.bfloat16)
    sp_count = lax.axis_size(SP)
    local_experts = specialist_gating_matrices.shape[0]
    experts = sp_count * local_experts
    picks = assigned_specialist_ids.shape[1]
    capacity = 2 * row_count * picks // experts
    own_ids = lax.dynamic_slice_in_dim(assigned_specialist_ids, tp_index * row_count, row_count, 0)
    sources, position = slot_tables(own_ids, 1, row_count, experts, capacity)
    own_position = position[0]
    outgoing = fetch_rows(expert_input, sources).reshape(
        sp_count, local_experts, 1, capacity, model_width
    )
    received = lax.all_to_all(outgoing, SP, split_axis=0, concat_axis=0, tiled=True)
    arrived = lax.all_gather(received, "tp", axis=2, tiled=True)
    gate_value = jnp.einsum(
        "slqcd,ldf->slqcf", arrived, specialist_gating_matrices, preferred_element_type=jnp.float32
    )
    up_value = jnp.einsum(
        "slqcd,ldf->slqcf", arrived, widening_matrices, preferred_element_type=jnp.float32
    )
    hidden = (jax.nn.silu(gate_value) * up_value).astype(jnp.bfloat16)
    partial_value = jnp.einsum(
        "slqcf,lfd->slqcd", hidden, contracting_matrices, preferred_element_type=jnp.float32
    )
    width_total = summed_on_arrival(partial_value.astype(jnp.bfloat16), "tp", 2).astype(
        jnp.bfloat16
    )
    returned = lax.all_to_all(width_total, SP, split_axis=0, concat_axis=0, tiled=True)
    answers = returned.reshape(experts * capacity, model_width)
    own_slots = own_ids.reshape(-1) * capacity + own_position
    gathered = (
        jnp.take(answers, own_slots, axis=0)
        .reshape(row_count, picks, model_width)
        .astype(jnp.float32)
    )
    lifted = jnp.exp(specialist_choice_affinity)
    shares = cluster_chance[:, None] * lifted / jnp.sum(lifted, axis=1, keepdims=True)
    return (middle_wide + jnp.sum(shares[:, :, None] * gathered, axis=1)).astype(jnp.bfloat16)


def solution(mesh):
    finer = Mesh(
        mesh.devices.reshape(mesh.shape["grp"], 16, 2, mesh.shape["tp"]),
        ("grp", "sp_0", "sp_1", "tp"),
    )
    return jax.shard_map(
        per_device,
        mesh=finer,
        in_specs=(
            P(GRP_SP_TP, None),
            P(GRP_SP, "tp"),
            P(GRP_SP, "tp"),
            P(GRP_SP, "tp"),
            P(GRP_SP, "tp"),
            P(GRP_SP, "tp"),
            P(GRP_SP, "tp"),
            P("tp"),
            P(None, "tp"),
            P(None, "tp"),
            P(None, "tp"),
            P(),
            P(),
            P(),
            P(SP, None, "tp"),
            P(SP, None, "tp"),
            P(SP, "tp", None),
            P(GRP_SP, None),
            P(GRP_SP_TP, None),
            P(GRP_SP_TP),
        ),
        out_specs=P(GRP_SP_TP, None),
        check_vma=False,
    )
```

profile of v0, /device:TPU:33, one launch (start us, length us, event | category | flops | bytes accessed | tf_op | source)
XLA Modules:
  0.0 418.4 jit_solution(9210774802349872012)
XLA Ops:
  7.4 5.7 %collective-permute-start.2 = (bf16[3,256]{1,0:T(4,128)(2,1)S(1)}, bf16[3,256]{1,0:T(4,128)(2,1)S(1)}, u32[]{:S(2)}, u32[]{:S(2)}) collective-permute-start(bf16[3,256]{1,0:T(4,128)(2,1)S(1)} %slice.211), channel_id=1, source_target_pairs={{0,4},{4,8},{8,12},{12,16},{16,20},{20,24},{24,28},{28,32},{32,36}... | collective-permute-start | bytes 4616 | tf_op jit(solution)/shard_map/ppermute | solution.py:46
  13.8 1.9 collective-permute-start
  17.1 4.8 %collective-permute-start.1 = (bf16[3,128]{1,0:T(4,128)(2,1)}, bf16[3,128]{1,0:T(4,128)(2,1)}, u32[]{:S(2)}, u32[]{:S(2)}) collective-permute-start(bf16[3,128]{1,0:T(4,128)(2,1)} %slice.202), channel_id=1, source_target_pairs={{0,4},{4,8},{8,12},{12,16},{16,20},{20,24},{24,28},{28,32},{32,36}... | collective-permute-start | bytes 2312 | tf_op jit(solution)/shard_map/ppermute | solution.py:46
  27.3 14.5 %all-reduce = bf16[8]{0:T(256)(128)(2,1)S(1)} all-reduce(bf16[8]{0:T(256)(128)(2,1)S(1)} %dynamic-update-slice), channel_id=2, replica_groups=mesh['grp'=2,'sp_0'=16,'sp_1'=2,'tp'=4] {'sp_1'}, use_global_device_ids=true, to_apply=%add | all-reduce | flops 8 | bytes 32
  49.6 5.7 %while.13 = (s32[]{:T(128)}, f32[1,4,64,128]{3,2,1,0:T(8,128)S(1)}, f32[4,1,4,64,128]{4,3,2,1,0:T(8,128)}, f32[4,1,4]{2,1,0:T(1,128)}, f32[4,1,4,64,128]{4,3,2,1,0:T(8,128)S(1)}, /*index=5*/s32[]{:T(128)}, s32[]{:T(128)}) while((s32[]{:T(128)}, f32[1,4,64,128]{3,2,1,0:T(8,128)S(1)}, f32[4,1,4,64,128]{4,3,2,1,0:T(8,128)}, ...), condition=%wide.region_2.3_spmd.clone, body=%wide.region_1.2_spmd.clone.sunk | while | flops 131075 | bytes 656016 | solution.py:101
  55.3 2.0 all-gather.1
  57.2 1.4 fusion.68
  60.6 25.0 %all_gather.22 = bf16[16,1,4]{2,1,0:T(2,128)(2,1)S(1)} all-gather(bf16[1,1,4]{2,1,0:T(2,128)(2,1)} %get-tuple-element.121), channel_id=1, replica_groups=mesh['grp'=2,'sp_0'=16,'sp_1'=2,'tp'=4] {'sp_0'}, dimensions={0}, use_global_device_ids=true | all-gather | bytes 136 | tf_op jit(solution)/shard_map/all_gather | solution.py:28
  91.8 24.7 %all-gather.5.cloned.1.call-done = bf16[16,1,4,64,128]{4,3,2,1,0:T(8,128)(2,1)} async-done(((bf16[1,1,4,64,128]{4,3,2,1,0:T(8,128)(2,1)}), bf16[16,1,4,64,128]{4,3,2,1,0:T(8,128)(2,1)}) %all-gather.5.cloned.1.call-update) | async-done | bytes 1048592 | tf_op jit(solution)/shard_map/all_gather | solution.py:28
  116.5 1.7 fusion.65
  118.2 1.5 fusion.21
  121.4 1.6 fusion.53
  123.0 4.0 all-to-all-start
  127.0 4.8 %all-to-all-done = bf16[4,64,256]{2,1,0:T(8,128)(2,1)S(1)} async-done(((bf16[4,64,256]{2,1,0:T(8,128)(2,1)}), bf16[4,64,256]{2,1,0:T(8,128)(2,1)S(1)}, u32[]{:S(2)}, u32[]{:S(2)}) %all-to-all-start) | async-done | bytes 131104 | tf_op jit(solution)/shard_map/all_to_all | solution.py:187
  132.1 3.2 multiply_reduce_fusion.1
  136.3 1.4 gather_fusion
  138.8 1.9 select_bitcast_fusion
  140.8 76.2 %all_to_all.28 = bf16[32,2,1,4,2048]{4,3,2,1,0:T(4,128)(2,1)S(1)} all-to-all(bf16[32,2,1,4,2048]{4,3,2,1,0:T(4,128)(2,1)S(1)} %select_bitcast_fusion), channel_id=1, replica_groups=mesh['grp'=2,'sp_0'=16,'sp_1'=2,'tp'=4] {'sp_0','sp_1'}, dimensions={0} | all-to-all | bytes 2097152 | tf_op jit(solution)/shard_map/all_to_all | solution.py:216
  217.0 1.6 copy.91
  218.6 44.0 %all-gather.7.cloned.1.call-done = bf16[32,2,4,4,2048]{4,0,3,2,1:T(8,128)(2,1)} async-done(((bf16[32,2,1,4,2048]{4,0,3,2,1:T(8,128)(2,1)}), bf16[32,2,4,4,2048]{4,0,3,2,1:T(8,128)(2,1)}) %all-gather.7.cloned.1.call-update) | async-done | bytes 4194320 | tf_op jit(solution)/shard_map/all_gather | solution.py:217
  262.6 4.1 fusion.9
  266.7 7.3 %convert_bitcast_fusion = bf16[4,32,2,1,4,2048]{5,1,4,0,2,3:T(8,128)(2,1)} fusion(bf16[2,256,2048]{2,1,0:T(8,128)(2,1)S(1)} %copy-done, bf16[32,2,4,4,2048]{4,0,3,2,1:T(8,128)(2,1)} %all-gather.7.cloned.1.call-done, bf16[2,2048,256]{2,1,0:T(8,128)(2,1)} %param.37, f32[32,2,4,4,256]{4,0,3,2,1:T(8,128)S(1)} %fusion.9), kind=kOutput, calls=%fused_computation.8 | convolution fusion | flops 2151153664 | bytes 13631488 | tf_op jit(solution)/shard_map/slqcf,lfd->slqcd/dot_general | solution.py:225
  274.0 2.5 copy.92
  276.5 51.3 %all_to_all.29 = bf16[4,32,2,1,4,2048]{5,1,4,2,3,0:T(8,128)(2,1)} all-to-all(bf16[4,32,2,1,4,2048]{5,1,4,2,3,0:T(8,128)(2,1)S(1)} %copy.92), channel_id=1, replica_groups=mesh['grp'=2,'sp_0'=16,'sp_1'=2,'tp'=4] {'tp'}, dimensions={0} | all-to-all | bytes 8388608 | tf_op jit(solution)/shard_map/all_to_all | solution.py:61
  327.8 3.1 reduce_sum.79
  330.9 1.9 copy.94
  332.8 14.3 %all-to-all-start.3 = ((bf16[32,2,1,4,2048]{4,3,1,2,0:T(4,128)(2,1)}), bf16[32,2,1,4,2048]{4,3,1,2,0:T(4,128)(2,1)}, u32[]{:S(2)}, u32[]{:S(2)}) async-start(bf16[32,2,1,4,2048]{4,3,1,2,0:T(4,128)(2,1)} %copy.94), calls=%async_computation.3 | async-start | bytes 2097152 | tf_op jit(solution)/shard_map/all_to_all | solution.py:231
  347.7 55.1 %all-to-all-done.3 = bf16[32,2,1,4,2048]{4,3,1,2,0:T(4,128)(2,1)} async-done(((bf16[32,2,1,4,2048]{4,3,1,2,0:T(4,128)(2,1)}), bf16[32,2,1,4,2048]{4,3,1,2,0:T(4,128)(2,1)}, u32[]{:S(2)}, u32[]{:S(2)}) %all-to-all-start.3) | async-done | bytes 1048608 | tf_op jit(solution)/shard_map/all_to_all | solution.py:231
  404.1 1.7 gather_fusion.1
  405.8 1.4 gather.15
  407.2 2.5 multiply_reduce_fusion
  409.7 1.8 add_convert_fusion
  (127 shorter events, 34.9 us)
Async XLA Ops:
  6.5 260.2 %copy-start = (bf16[2,256,2048]{2,1,0:T(8,128)(2,1)S(1)}, bf16[2,256,2048]{2,1,0:T(8,128)(2,1)}, u32[]{:S(2)}) copy-start(bf16[2,256,2048]{2,1,0:T(8,128)(2,1)} %param.38) | copy-start | bytes 6291460
  6.6 109.9 %all-gather.5.cloned.1.call-start = ((), (), s32[]{:S(2)}) async-start(), calls=%async_computation.4 | async-start | bytes 1114112 | tf_op jit(solution)/shard_map/all_gather | solution.py:28
  7.4 40.4 %collective-permute-start.2 = (bf16[3,256]{1,0:T(4,128)(2,1)S(1)}, bf16[3,256]{1,0:T(4,128)(2,1)S(1)}, u32[]{:S(2)}, u32[]{:S(2)}) collective-permute-start(bf16[3,256]{1,0:T(4,128)(2,1)S(1)} %slice.211), channel_id=1, source_target_pairs={{0,4},{4,8},{8,12},{12,16},{16,20},{20,24},{24,28},{28,32},{32,36}... | collective-permute-start | bytes 4616 | tf_op jit(solution)/shard_map/ppermute | solution.py:46
  13.8 33.0 %collective-permute-start = (bf16[3,128]{1,0:T(4,128)(2,1)S(1)}, bf16[3,128]{1,0:T(4,128)(2,1)S(1)}, u32[]{:S(2)}, u32[]{:S(2)}) collective-permute-start(bf16[3,128]{1,0:T(4,128)(2,1)S(1)} %slice.193), channel_id=1, source_target_pairs={{0,4},{4,8},{8,12},{12,16},{16,20},{20,24},{24,28},{28,32},{32,36}... | collective-permute-start | bytes 2312 | tf_op jit(solution)/shard_map/ppermute | solution.py:46
  17.1 73.7 %collective-permute-start.1 = (bf16[3,128]{1,0:T(4,128)(2,1)}, bf16[3,128]{1,0:T(4,128)(2,1)}, u32[]{:S(2)}, u32[]{:S(2)}) collective-permute-start(bf16[3,128]{1,0:T(4,128)(2,1)} %slice.202), channel_id=1, source_target_pairs={{0,4},{4,8},{8,12},{12,16},{16,20},{20,24},{24,28},{28,32},{32,36}... | collective-permute-start | bytes 2312 | tf_op jit(solution)/shard_map/ppermute | solution.py:46
  24.3 24.4 %copy-start.6 = (f32[4,1,1,4]{3,2,1,0:T(1,128)}, f32[4,1,1,4]{3,2,1,0:T(1,128)S(1)}, u32[]{:S(2)}) copy-start(f32[4,1,1,4]{3,2,1,0:T(1,128)S(1)} %get-tuple-element.89) | copy-start | bytes 196
  43.2 3.5 copy-start.7
  43.9 4.9 %copy-start.11 = (s32[128]{0:T(128)}, s32[128]{0:T(128)S(1)}, u32[]{:S(2)}) copy-start(s32[128]{0:T(128)S(1)} %select_reduce_fusion) | copy-start | bytes 1540
  48.8 42.0 %copy-start.3 = (bf16[256,128]{1,0:T(8,128)(2,1)S(1)}, bf16[256,128]{1,0:T(8,128)(2,1)}, u32[]{:S(2)}) copy-start(bf16[256,128]{1,0:T(8,128)(2,1)} %param.26) | copy-start | bytes 196612
  91.7 40.4 %copy-start.2 = (bf16[64,2048]{1,0:T(8,128)(2,1)S(1)}, bf16[64,2048]{1,0:T(8,128)(2,1)}, u32[]{:S(2)}) copy-start(bf16[64,2048]{1,0:T(8,128)(2,1)} %param.22) | copy-start | bytes 786436
  91.7 40.4 %copy-start.10 = (f32[1024]{0:T(1024)S(1)}, f32[1024]{0:T(1024)}, u32[]{:S(2)}) copy-start(f32[1024]{0:T(1024)} %param.33) | copy-start | bytes 12292
  121.0 15.1 %copy-start.9 = (f32[2048]{0:T(1024)S(1)}, f32[2048]{0:T(1024)}, u32[]{:S(2)}) copy-start(f32[2048]{0:T(1024)} %param.35) | copy-start | bytes 24580
  123.0 8.8 %all-to-all-start = ((bf16[4,64,256]{2,1,0:T(8,128)(2,1)}), bf16[4,64,256]{2,1,0:T(8,128)(2,1)S(1)}, u32[]{:S(2)}, u32[]{:S(2)}) async-start(bf16[4,64,256]{2,1,0:T(8,128)(2,1)} %bitcast.53), calls=%async_computation | async-start | bytes 262144 | tf_op jit(solution)/shard_map/all_to_all | solution.py:187
  127.0 135.6 %all-gather.7.cloned.1.call-start = ((), (), s32[]{:S(2)}) async-start(), calls=%async_computation.5 | async-start | bytes 5242880 | tf_op jit(solution)/shard_map/all_gather | solution.py:217
  135.3 0.8 copy-start.1
  136.2 2.6 copy-start.4
  136.2 2.6 copy-start.5
  327.8 19.3 %copy-start.12 = (s32[128]{0:T(128)S(1)}, s32[128]{0:T(128)}, u32[]{:S(2)}) copy-start(s32[128]{0:T(128)} %copy-done.11) | copy-start | bytes 1540
  327.8 19.5 %copy-start.8 = (s32[64,2]{0,1:T(2,128)S(1)}, s32[64,2]{0,1:T(2,128)}, u32[]{:S(2)}) copy-start(s32[64,2]{0,1:T(2,128)} %copy-done.7) | copy-start | bytes 1540
  327.8 19.7 %copy-start.13 = (f32[64,2]{0,1:T(2,128)S(1)}, f32[64,2]{0,1:T(2,128)}, u32[]{:S(2)}) copy-start(f32[64,2]{0,1:T(2,128)} %param.40) | copy-start | bytes 1540
  327.8 19.7 %copy-start.15 = (f32[64]{0:T(128)S(1)}, f32[64]{0:T(128)}, u32[]{:S(2)}) copy-start(f32[64]{0:T(128)} %param.41) | copy-start | bytes 772
  327.8 19.8 %copy-start.14 = (s32[128]{0:T(128)S(1)}, s32[128]{0:T(128)}, u32[]{:S(2)}) copy-start(s32[128]{0:T(128)} %fusion.70) | copy-start | bytes 1540
  332.8 69.9 %all-to-all-start.3 = ((bf16[32,2,1,4,2048]{4,3,1,2,0:T(4,128)(2,1)}), bf16[32,2,1,4,2048]{4,3,1,2,0:T(4,128)(2,1)}, u32[]{:S(2)}, u32[]{:S(2)}) async-start(bf16[32,2,1,4,2048]{4,3,1,2,0:T(4,128)(2,1)} %copy.94), calls=%async_computation.3 | async-start | bytes 2097152 | tf_op jit(solution)/shard_map/all_to_all | solution.py:231
Sparse Core Ops, SparseCore 0:
  58.8 57.6 all-gather.4
  218.7 43.8 all-gather.6
where the time goes:
time: 420 us; the launch traced here: 418 us
  blocking collectives  169 us (40%)
  waiting for transfers between devices  129 us (31%)
  starting transfers between devices  30.8 us (7%)
  local copies, waits for them, and re-layouts  29.3 us (7%)
  other arithmetic  28.5 us (7%)
  matrix products  17.5 us (4%)
  between operations  14.6 us (3%)
    all_to_all x1, blocking collectives, per_device(): lax.all_to_all(outgoing, SP, split_axis=0, concat_axis=0, tiled=True)  76.2 us
    all_to_all x1, waiting for transfers between devices, per_device(): lax.all_to_all(width_total, SP, split_axis=0, concat_axis=0, tiled=True)  55.1 us
    all_to_all x1, blocking collectives, summed_on_arrival(): blocks = lax.all_to_all(split_up(x, dim, size), axis, 0, 0, tiled=True)  51.3 us
    all_gather x1, waiting for transfers between devices, per_device(): arrived = lax.all_gather(received, 'tp', axis=2, tiled=True)  44 us
    all_gather x2, blocking collectives, carried_in(): lax.all_gather(part.astype(kind), axis)  26.9 us
    all_gather x1, waiting for transfers between devices, carried_in(): lax.all_gather(part.astype(kind), axis)  24.7 us
    unnamed x1, blocking collectives  14.5 us
    all_to_all x1, starting transfers between devices, per_device(): lax.all_to_all(width_total, SP, split_axis=0, concat_axis=0, tiled=True)  14.3 us
  transfers between devices with their start and end apart: 7, of which 4 were waited for; matrix products, arithmetic and copies ran while one was open for 7% of the time, Pallas kernels for 0%

commit v1 on v0

--- a/solution.py
+++ b/solution.py
@@ -214,7 +214,30 @@
         sp_count, local_experts, 1, capacity, model_width
     )
     received = lax.all_to_all(outgoing, SP, split_axis=0, concat_axis=0, tiled=True)
-    arrived = lax.all_gather(received, "tp", axis=2, tiled=True)
+    f_now, now, outer = (lax.axis_size("tp"), lax.axis_index("tp"), received.shape[2])
+    arrived = lax.dynamic_update_slice_in_dim(
+        jnp.zeros(
+            [p * f_now if rr == 2 else p for rr, p in enumerate(received.shape)], received.dtype
+        ),
+        received,
+        now * outer,
+        axis=2,
+    )
+    moved = n_now = received
+    for dev_j in range(1, f_now // 2 + 1):
+        moved = lax.ppermute(
+            moved, axis_name="tp", perm=[(rr, (rr + 1) % f_now) for rr in range(f_now)]
+        )
+        arrived = lax.dynamic_update_slice_in_dim(
+            arrived, moved, (now - dev_j) % f_now * outer, axis=2
+        )
+        if 2 * dev_j < f_now:
+            n_now = lax.ppermute(
+                n_now, axis_name="tp", perm=[(rr, (rr - 1) % f_now) for rr in range(f_now)]
+            )
+            arrived = lax.dynamic_update_slice_in_dim(
+                arrived, n_now, (now + dev_j) % f_now * outer, axis=2
+            )
     gate_value = jnp.einsum(
         "slqcd,ldf->slqcf", arrived, specialist_gating_matrices, preferred_element_type=jnp.float32
     )

time: 420 us -> 416 us (level)
  local copies, waits for them, and re-layouts: 29.3 us -> 35.2 us
    all_gather x1 -> x0, waiting for transfers between devices: 44 us -> none  [per_device(): arrived = lax.all_gather(received, 'tp', axis=2, tiled=True)]
    ppermute x0 -> x3, waiting for transfers between devices: none -> 42.7 us  [the longest x2 42.7 us: per_device(): lax.ppermute(moved, axis_name='tp', perm=[(rr, (rr + 1) % f_now) for rr i...]
    all_to_all x1, starting transfers between devices: 14.3 us -> 7.78 us  [per_device(): lax.all_to_all(width_total, SP, split_axis=0, concat_axis=0, tiled=True)]
    dynamic_update_slice x0 -> x4, local copies, waits for them, and re-layouts: none -> 5.01 us  [the longest x2 2.5 us: per_device(): lax.dynamic_update_slice_in_dim(arrived, moved, (now - dev_j) % f_now * o...]
  transfers between devices with their start and end apart: 7 -> 9, of which waited for: 4 -> 5; matrix products, arithmetic and copies ran while one was open for 7% -> 8% of each run, Pallas kernels for 0% -> 0%
where the time goes in v1:
time: 416 us; the launch traced here: 415 us
  blocking collectives  167 us (40%)
  waiting for transfers between devices  128 us (31%)
  local copies, waits for them, and re-layouts  35.2 us (8%)
  other arithmetic  28.5 us (7%)
  starting transfers between devices  27.2 us (7%)
  matrix products  14.7 us (4%)
  between operations  14.6 us (4%)
    all_to_all x1, blocking collectives, per_device(): lax.all_to_all(outgoing, SP, split_axis=0, concat_axis=0, tiled=True)  76 us
    all_to_all x1, waiting for transfers between devices, per_device(): lax.all_to_all(width_total, SP, split_axis=0, concat_axis=0, tiled=True)  55.2 us
    all_to_all x1, blocking collectives, summed_on_arrival(): blocks = lax.all_to_all(split_up(x, dim, size), axis, 0, 0, tiled=True)  49.9 us
    ppermute x2, waiting for transfers between devices, per_device(): lax.ppermute(moved, axis_name='tp', perm=[(rr, (rr + 1) % f_now) for rr i...  42.7 us
    all_gather x2, blocking collectives, carried_in(): lax.all_gather(part.astype(kind), axis)  26.5 us
    all_gather x1, waiting for transfers between devices, carried_in(): lax.all_gather(part.astype(kind), axis)  25.3 us
    unnamed x1, blocking collectives  14.5 us
    ppermute x3, starting transfers between devices, from_behind(): return lax.ppermute(x, axis, pairs)  12.5 us
  transfers between devices with their start and end apart: 9, of which 5 were waited for; matrix products, arithmetic and copies ran while one was open for 8% of the time, Pallas kernels for 0%

profile of v1, /device:TPU:33, one launch (start us, length us, event | category | flops | bytes accessed | tf_op | source)
XLA Modules:
  0.0 415.1 jit_solution(1676475671434838788)
XLA Ops:
  7.4 5.7 %collective-permute-start.2 = (bf16[3,256]{1,0:T(4,128)(2,1)S(1)}, bf16[3,256]{1,0:T(4,128)(2,1)S(1)}, u32[]{:S(2)}, u32[]{:S(2)}) collective-permute-start(bf16[3,256]{1,0:T(4,128)(2,1)S(1)} %slice.211), channel_id=1, source_target_pairs={{0,4},{4,8},{8,12},{12,16},{16,20},{20,24},{24,28},{28,32},{32,36}... | collective-permute-start | bytes 4616 | tf_op jit(solution)/shard_map/ppermute | solution.py:46
  13.8 1.9 collective-permute-start
  17.1 4.8 %collective-permute-start.1 = (bf16[3,128]{1,0:T(4,128)(2,1)}, bf16[3,128]{1,0:T(4,128)(2,1)}, u32[]{:S(2)}, u32[]{:S(2)}) collective-permute-start(bf16[3,128]{1,0:T(4,128)(2,1)} %slice.202), channel_id=1, source_target_pairs={{0,4},{4,8},{8,12},{12,16},{16,20},{20,24},{24,28},{28,32},{32,36}... | collective-permute-start | bytes 2312 | tf_op jit(solution)/shard_map/ppermute | solution.py:46
  27.4 14.5 %all-reduce = bf16[8]{0:T(256)(128)(2,1)S(1)} all-reduce(bf16[8]{0:T(256)(128)(2,1)S(1)} %dynamic-update-slice), channel_id=2, replica_groups=mesh['grp'=2,'sp_0'=16,'sp_1'=2,'tp'=4] {'sp_1'}, use_global_device_ids=true, to_apply=%add | all-reduce | flops 8 | bytes 32
  49.8 5.7 %while.13 = (s32[]{:T(128)}, f32[1,4,64,128]{3,2,1,0:T(8,128)S(1)}, f32[4,1,4,64,128]{4,3,2,1,0:T(8,128)}, f32[4,1,4]{2,1,0:T(1,128)}, f32[4,1,4,64,128]{4,3,2,1,0:T(8,128)S(1)}, /*index=5*/s32[]{:T(128)}, s32[]{:T(128)}) while((s32[]{:T(128)}, f32[1,4,64,128]{3,2,1,0:T(8,128)S(1)}, f32[4,1,4,64,128]{4,3,2,1,0:T(8,128)}, ...), condition=%wide.region_2.3_spmd.clone, body=%wide.region_1.2_spmd.clone.sunk | while | flops 131075 | bytes 656016 | solution.py:101
  55.4 2.0 all-gather.1
  60.8 24.6 %all_gather.19 = bf16[16,1,4]{2,1,0:T(2,128)(2,1)S(1)} all-gather(bf16[1,1,4]{2,1,0:T(2,128)(2,1)} %get-tuple-element.121), channel_id=1, replica_groups=mesh['grp'=2,'sp_0'=16,'sp_1'=2,'tp'=4] {'sp_0'}, dimensions={0}, use_global_device_ids=true | all-gather | bytes 136 | tf_op jit(solution)/shard_map/all_gather | solution.py:28
  91.4 25.3 %all-gather.4.cloned.1.call-done = bf16[16,1,4,64,128]{4,3,2,1,0:T(8,128)(2,1)} async-done(((bf16[1,1,4,64,128]{4,3,2,1,0:T(8,128)(2,1)}), bf16[16,1,4,64,128]{4,3,2,1,0:T(8,128)(2,1)}) %all-gather.4.cloned.1.call-update) | async-done | bytes 1048592 | tf_op jit(solution)/shard_map/all_gather | solution.py:28
  116.7 1.7 fusion.62
  118.3 1.5 fusion.15
  121.6 1.6 fusion.50
  123.2 4.2 %all-to-all-start = ((bf16[4,64,256]{2,1,0:T(8,128)(2,1)}), bf16[4,64,256]{2,1,0:T(8,128)(2,1)S(1)}, u32[]{:S(2)}, u32[]{:S(2)}) async-start(bf16[4,64,256]{2,1,0:T(8,128)(2,1)} %bitcast.53), calls=%async_computation | async-start | bytes 262144 | tf_op jit(solution)/shard_map/all_to_all | solution.py:187
  127.4 4.8 %all-to-all-done = bf16[4,64,256]{2,1,0:T(8,128)(2,1)S(1)} async-done(((bf16[4,64,256]{2,1,0:T(8,128)(2,1)}), bf16[4,64,256]{2,1,0:T(8,128)(2,1)S(1)}, u32[]{:S(2)}, u32[]{:S(2)}) %all-to-all-start) | async-done | bytes 131104 | tf_op jit(solution)/shard_map/all_to_all | solution.py:187
  132.5 3.2 multiply_reduce_fusion.1
  139.3 1.9 fusion.17
  141.2 76.0 %all_to_all.28 = bf16[32,2,1,4,2048]{4,3,2,1,0:T(4,128)(2,1)S(1)} all-to-all(bf16[32,2,1,4,2048]{4,3,2,1,0:T(4,128)(2,1)S(1)} %fusion.17), channel_id=1, replica_groups=mesh['grp'=2,'sp_0'=16,'sp_1'=2,'tp'=4] {'sp_0','sp_1'}, dimensions={0} | all-to-all | bytes 2097152 | tf_op jit(solution)/shard_map/all_to_all | solution.py:216
  217.4 2.4 collective-permute-start.4
  219.8 22.8 %collective-permute-done.3 = bf16[32,2,1,4,2048]{4,3,2,1,0:T(4,128)(2,1)} collective-permute-done((bf16[32,2,1,4,2048]{4,3,2,1,0:T(4,128)(2,1)S(1)}, bf16[32,2,1,4,2048]{4,3,2,1,0:T(4,128)(2,1)}, u32[]{:S(2)}, u32[]{:S(2)}) %collective-permute-start.3) | collective-permute-done | bytes 1048608 | tf_op jit(solution)/shard_map/ppermute | solution.py:228
  243.8 1.9 copy_dynamic-update-slice_fusion.2
  245.7 1.9 copy_dynamic-update-slice_fusion.1
  247.6 19.8 %collective-permute-done.5 = bf16[32,2,1,4,2048]{4,3,2,1,0:T(4,128)(2,1)S(1)} collective-permute-done((bf16[32,2,1,4,2048]{4,3,2,1,0:T(4,128)(2,1)}, bf16[32,2,1,4,2048]{4,3,2,1,0:T(4,128)(2,1)S(1)}, u32[]{:S(2)}, u32[]{:S(2)}) %collective-permute-start.5) | collective-permute-done | bytes 1048608 | tf_op jit(solution)/shard_map/ppermute | solution.py:228
  268.1 1.9 copy-done.2
  271.3 7.3 %convert_bitcast_fusion = bf16[4,32,2,1,4,2048]{5,1,4,0,2,3:T(8,128)(2,1)} fusion(bf16[2,256,2048]{2,1,0:T(8,128)(2,1)S(1)} %copy-done, f32[32,2,4,4,256]{4,0,3,2,1:T(8,128)S(1)} %fusion.9, bf16[32,2,4,4,2048]{4,0,3,2,1:T(8,128)(2,1)} %copy-done.2, bf16[2,2048,256]{2,1,0:T(8,128)(2,1)} %param.37), kind=kOutput, calls=%fused_computation.8 | convolution fusion | flops 2151153664 | bytes 13631488 | tf_op jit(solution)/shard_map/slqcf,lfd->slqcd/dot_general | solution.py:248
  278.6 2.5 copy.99
  281.1 49.9 %all_to_all.29 = bf16[4,32,2,1,4,2048]{5,1,4,2,3,0:T(8,128)(2,1)} all-to-all(bf16[4,32,2,1,4,2048]{5,1,4,2,3,0:T(8,128)(2,1)S(1)} %copy.99), channel_id=1, replica_groups=mesh['grp'=2,'sp_0'=16,'sp_1'=2,'tp'=4] {'tp'}, dimensions={0} | all-to-all | bytes 8388608 | tf_op jit(solution)/shard_map/all_to_all | solution.py:61
  331.0 3.1 reduce_sum.79
  334.1 1.8 copy.101
  335.9 7.8 %all-to-all-start.3 = ((bf16[32,2,1,4,2048]{4,3,1,2,0:T(4,128)(2,1)}), bf16[32,2,1,4,2048]{4,3,1,2,0:T(4,128)(2,1)}, u32[]{:S(2)}, u32[]{:S(2)}) async-start(bf16[32,2,1,4,2048]{4,3,1,2,0:T(4,128)(2,1)} %copy.101), calls=%async_computation.3 | async-start | bytes 2097152 | tf_op jit(solution)/shard_map/all_to_all | solution.py:254
  344.2 55.2 %all-to-all-done.3 = bf16[32,2,1,4,2048]{4,3,1,2,0:T(4,128)(2,1)} async-done(((bf16[32,2,1,4,2048]{4,3,1,2,0:T(4,128)(2,1)}), bf16[32,2,1,4,2048]{4,3,1,2,0:T(4,128)(2,1)}, u32[]{:S(2)}, u32[]{:S(2)}) %all-to-all-start.3) | async-done | bytes 1048608 | tf_op jit(solution)/shard_map/all_to_all | solution.py:254
  400.7 1.7 gather_fusion.1
  403.8 2.5 multiply_reduce_fusion
  406.4 1.8 add_convert_fusion
  (138 shorter events, 42.3 us)
Async XLA Ops:
  6.5 264.7 %copy-start = (bf16[2,256,2048]{2,1,0:T(8,128)(2,1)S(1)}, bf16[2,256,2048]{2,1,0:T(8,128)(2,1)}, u32[]{:S(2)}) copy-start(bf16[2,256,2048]{2,1,0:T(8,128)(2,1)} %param.38) | copy-start | bytes 6291460
  6.6 110.1 %all-gather.4.cloned.1.call-start = ((), (), s32[]{:S(2)}) async-start(), calls=%async_computation.4 | async-start | bytes 1114112 | tf_op jit(solution)/shard_map/all_gather | solution.py:28
  7.4 40.5 %collective-permute-start.2 = (bf16[3,256]{1,0:T(4,128)(2,1)S(1)}, bf16[3,256]{1,0:T(4,128)(2,1)S(1)}, u32[]{:S(2)}, u32[]{:S(2)}) collective-permute-start(bf16[3,256]{1,0:T(4,128)(2,1)S(1)} %slice.211), channel_id=1, source_target_pairs={{0,4},{4,8},{8,12},{12,16},{16,20},{20,24},{24,28},{28,32},{32,36}... | collective-permute-start | bytes 4616 | tf_op jit(solution)/shard_map/ppermute | solution.py:46
  13.8 33.1 %collective-permute-start = (bf16[3,128]{1,0:T(4,128)(2,1)S(1)}, bf16[3,128]{1,0:T(4,128)(2,1)S(1)}, u32[]{:S(2)}, u32[]{:S(2)}) collective-permute-start(bf16[3,128]{1,0:T(4,128)(2,1)S(1)} %slice.193), channel_id=1, source_target_pairs={{0,4},{4,8},{8,12},{12,16},{16,20},{20,24},{24,28},{28,32},{32,36}... | collective-permute-start | bytes 2312 | tf_op jit(solution)/shard_map/ppermute | solution.py:46
  17.1 73.3 %collective-permute-start.1 = (bf16[3,128]{1,0:T(4,128)(2,1)}, bf16[3,128]{1,0:T(4,128)(2,1)}, u32[]{:S(2)}, u32[]{:S(2)}) collective-permute-start(bf16[3,128]{1,0:T(4,128)(2,1)} %slice.202), channel_id=1, source_target_pairs={{0,4},{4,8},{8,12},{12,16},{16,20},{20,24},{24,28},{28,32},{32,36}... | collective-permute-start | bytes 2312 | tf_op jit(solution)/shard_map/ppermute | solution.py:46
  24.3 24.5 %copy-start.7 = (f32[4,1,1,4]{3,2,1,0:T(1,128)}, f32[4,1,1,4]{3,2,1,0:T(1,128)S(1)}, u32[]{:S(2)}) copy-start(f32[4,1,1,4]{3,2,1,0:T(1,128)S(1)} %get-tuple-element.89) | copy-start | bytes 196
  43.3 3.6 copy-start.8
  44.0 4.9 %copy-start.12 = (s32[128]{0:T(128)}, s32[128]{0:T(128)S(1)}, u32[]{:S(2)}) copy-start(s32[128]{0:T(128)S(1)} %select_reduce_fusion) | copy-start | bytes 1540
  48.9 41.4 %copy-start.4 = (bf16[256,128]{1,0:T(8,128)(2,1)S(1)}, bf16[256,128]{1,0:T(8,128)(2,1)}, u32[]{:S(2)}) copy-start(bf16[256,128]{1,0:T(8,128)(2,1)} %param.26) | copy-start | bytes 196612
  91.3 41.2 %copy-start.3 = (bf16[64,2048]{1,0:T(8,128)(2,1)S(1)}, bf16[64,2048]{1,0:T(8,128)(2,1)}, u32[]{:S(2)}) copy-start(bf16[64,2048]{1,0:T(8,128)(2,1)} %param.22) | copy-start | bytes 786436
  91.3 41.2 %copy-start.11 = (f32[1024]{0:T(1024)S(1)}, f32[1024]{0:T(1024)}, u32[]{:S(2)}) copy-start(f32[1024]{0:T(1024)} %param.33) | copy-start | bytes 12292
  121.2 15.3 %copy-start.10 = (f32[2048]{0:T(1024)S(1)}, f32[2048]{0:T(1024)}, u32[]{:S(2)}) copy-start(f32[2048]{0:T(1024)} %param.35) | copy-start | bytes 24580
  123.2 9.1 %all-to-all-start = ((bf16[4,64,256]{2,1,0:T(8,128)(2,1)}), bf16[4,64,256]{2,1,0:T(8,128)(2,1)S(1)}, u32[]{:S(2)}, u32[]{:S(2)}) async-start(bf16[4,64,256]{2,1,0:T(8,128)(2,1)} %bitcast.53), calls=%async_computation | async-start | bytes 262144 | tf_op jit(solution)/shard_map/all_to_all | solution.py:187
  135.7 0.8 copy-start.1
  136.6 2.6 copy-start.5
  136.7 2.6 copy-start.6
  217.1 25.5 %collective-permute-start.3 = (bf16[32,2,1,4,2048]{4,3,2,1,0:T(4,128)(2,1)S(1)}, bf16[32,2,1,4,2048]{4,3,2,1,0:T(4,128)(2,1)}, u32[]{:S(2)}, u32[]{:S(2)}) collective-permute-start(bf16[32,2,1,4,2048]{4,3,2,1,0:T(4,128)(2,1)S(1)} %all_to_all.28), channel_id=1, source_target_pairs={{0,1},{1,2},{2,3},{3,0},{4,5},{5,6},{6,7},{7,4},{8,9},{9,10},{10,1... | collective-permute-start | bytes 3145736 | tf_op jit(solution)/shard_map/ppermute | solution.py:228
  217.4 28.3 %collective-permute-start.4 = (bf16[32,2,1,4,2048]{4,3,2,1,0:T(4,128)(2,1)S(1)}, bf16[32,2,1,4,2048]{4,3,2,1,0:T(4,128)(2,1)}, u32[]{:S(2)}, u32[]{:S(2)}) collective-permute-start(bf16[32,2,1,4,2048]{4,3,2,1,0:T(4,128)(2,1)S(1)} %all_to_all.28), channel_id=1, source_target_pairs={{0,3},{1,0},{2,1},{3,2},{4,7},{5,4},{6,5},{7,6},{8,11},{9,8},{10,9... | collective-permute-start | bytes 3145736 | tf_op jit(solution)/shard_map/ppermute | solution.py:235
  242.7 24.8 %collective-permute-start.5 = (bf16[32,2,1,4,2048]{4,3,2,1,0:T(4,128)(2,1)}, bf16[32,2,1,4,2048]{4,3,2,1,0:T(4,128)(2,1)S(1)}, u32[]{:S(2)}, u32[]{:S(2)}) collective-permute-start(bf16[32,2,1,4,2048]{4,3,2,1,0:T(4,128)(2,1)} %collective-permute-done.3), channel_id=1, source_target_pairs={{0,1},{1,2},{2,3},{3,0},{4,5},{5,6},{6,7},{7,4},{8,9},{9,10},{10,1... | collective-permute-start | bytes 3145736 | tf_op jit(solution)/shard_map/ppermute | solution.py:228
  243.2 26.8 %copy-start.17 = (bf16[2,2048,256]{2,1,0:T(8,128)(2,1)S(1)}, bf16[2,2048,256]{2,1,0:T(8,128)(2,1)}, u32[]{:S(2)}) copy-start(bf16[2,2048,256]{2,1,0:T(8,128)(2,1)} %param.36) | copy-start | bytes 6291460
  268.1 1.9 copy-start.2
  331.0 12.7 %copy-start.13 = (s32[128]{0:T(128)S(1)}, s32[128]{0:T(128)}, u32[]{:S(2)}) copy-start(s32[128]{0:T(128)} %copy-done.12) | copy-start | bytes 1540
  331.0 13.0 %copy-start.9 = (s32[64,2]{0,1:T(2,128)S(1)}, s32[64,2]{0,1:T(2,128)}, u32[]{:S(2)}) copy-start(s32[64,2]{0,1:T(2,128)} %copy-done.8) | copy-start | bytes 1540
  331.0 13.1 %copy-start.14 = (f32[64,2]{0,1:T(2,128)S(1)}, f32[64,2]{0,1:T(2,128)}, u32[]{:S(2)}) copy-start(f32[64,2]{0,1:T(2,128)} %param.40) | copy-start | bytes 1540
  331.0 13.1 %copy-start.16 = (f32[64]{0:T(128)S(1)}, f32[64]{0:T(128)}, u32[]{:S(2)}) copy-start(f32[64]{0:T(128)} %param.41) | copy-start | bytes 772
  331.0 13.2 %copy-start.15 = (s32[128]{0:T(128)S(1)}, s32[128]{0:T(128)}, u32[]{:S(2)}) copy-start(s32[128]{0:T(128)} %fusion.67) | copy-start | bytes 1540
  335.9 63.5 %all-to-all-start.3 = ((bf16[32,2,1,4,2048]{4,3,1,2,0:T(4,128)(2,1)}), bf16[32,2,1,4,2048]{4,3,1,2,0:T(4,128)(2,1)}, u32[]{:S(2)}, u32[]{:S(2)}) async-start(bf16[32,2,1,4,2048]{4,3,1,2,0:T(4,128)(2,1)} %copy.101), calls=%async_computation.3 | async-start | bytes 2097152 | tf_op jit(solution)/shard_map/all_to_all | solution.py:254
Sparse Core Ops, SparseCore 0:
  59.0 57.6 all-gather.3
